TPU v7x, 32 devices: a whole 2x2x4 slice. The times are simulated.
32 devices in a mesh: fs: 8 (over z, x), tp: 4 (over y, core).
Axes of the slice: x: 2, y: 2, z: 4, core: 2. Of those that a mesh axis runs over, the one named last changes fastest.
Arguments:
- tokens: bfloat16 [8192, 2048], P('fs', 'tp'), may hold values from -17 to 17
- first_gain: float32 [2048], replicated, may hold values from 0.1 to 1.9
- first_gate: bfloat16 [2048, 5120], P('fs', 'tp'), may hold values from -0.125 to 0.125
- first_up: bfloat16 [2048, 5120], P('fs', 'tp'), may hold values from -0.125 to 0.125
- first_down: bfloat16 [2048, 5120], P('fs', 'tp'), may hold values from -0.078125 to 0.078125
- mix_gain: float32 [2048], replicated, may hold values from 0.1 to 1.9
- mix_input: bfloat16 [2048, 1024], P('fs', 'tp'), may hold values from -0.125 to 0.125
- mix_branch: bfloat16 [2048, 1024], P('fs', 'tp'), may hold values from -0.125 to 0.125
- conv_weight: bfloat16 [4, 1024], P(None, 'tp'), may hold values from -3 to 3
- rate_weight: bfloat16 [16, 64, 64], P('tp'), may hold values from -0.75 to 0.75
- input_weight: bfloat16 [16, 64, 64], P('tp'), may hold values from -0.75 to 0.75
- decay_param: float32 [1024], P('tp'), may hold values from 3 to 11
- decay_shift: float32 [8192, 16], P('fs', 'tp'), may hold values from -1.5 to 0
- mix_output: bfloat16 [2048, 1024], P('fs', 'tp'), may hold values from -0.1875 to 0.1875
- second_gain: float32 [2048], replicated, may hold values from 0.1 to 1.9
- second_gate: bfloat16 [2048, 5120], P('fs', 'tp'), may hold values from -0.125 to 0.125
- second_up: bfloat16 [2048, 5120], P('fs', 'tp'), may hold values from -0.125 to 0.125
- second_down: bfloat16 [2048, 5120], P('fs', 'tp'), may hold values from -0.078125 to 0.078125
- final_gain: float32 [2048], P('tp'), may hold values from 0.1 to 1.9
Outputs:
- output: bfloat16 [8192, 2048], P('fs', 'tp')
All inputs are finite; a program needn't handle non-finite values.
Results may differ from a plain program's by a relative error of at most 0.019.
Values may be sent and summed in bfloat16 or wider, within the bound.
A program may use at most 128 MiB of HBM per device.

v0:
```python
import jax
import jax.numpy as jnp
from jax import lax
from jax.sharding import PartitionSpec as P

D = 2048
HEAD_DIM = 64
CONV = 4
SEQ = 1024


norm_eps = 1e-06
rate_scale = 8.0


def rms_rows(rows, gain):
    values = rows.astype(jnp.float32)
    scale = lax.rsqrt(jnp.mean(values * values, axis=-1, keepdims=True) + norm_eps)
    return (values * scale * gain).astype(jnp.bfloat16)


def full_rows(stream, gain):
    whole = lax.all_gather(stream, "tp", axis=1, tiled=True)
    return rms_rows(whole, gain)


def reduce_back(partial_value):
    return lax.psum_scatter(
        partial_value.astype(jnp.bfloat16), "tp", scatter_dimension=1, tiled=True
    ).astype(jnp.float32)


def contract_last(left, right):
    return lax.dot_general(
        left, right, (((1,), (1,)), ((), ())), preferred_element_type=jnp.float32
    )


def half_step(stream, gain, weight_gate, weight_up, weight_down):
    normed = full_rows(stream, gain)
    whole_gate, whole_up, whole_down = (
        lax.all_gather(weight_gate, "fs", axis=0, tiled=True),
        lax.all_gather(weight_up, "fs", axis=0, tiled=True),
        lax.all_gather(weight_down, "fs", axis=0, tiled=True),
    )
    gate_value = jnp.dot(normed, whole_gate, preferred_element_type=jnp.float32)
    up_value = jnp.dot(normed, whole_up, preferred_element_type=jnp.float32)
    hidden = (jax.nn.silu(gate_value) * up_value).astype(jnp.bfloat16)
    partial_value = contract_last(hidden, whole_down)
    total = reduce_back(partial_value)
    return (stream.astype(jnp.float32) + 0.5 * total).astype(jnp.bfloat16)


def combine_steps(earlier, later):
    return (earlier[0] * later[0], later[0] * earlier[1] + later[1])


def lane_mixer(
    stream,
    gain,
    mix_input,
    mix_branch,
    conv_weight,
    rate_weight,
    input_weight,
    decay_param,
    decay_shift,
    mix_output,
):
    normed = full_rows(stream, gain)
    whole_input, whole_branch, whole_output = (
        lax.all_gather(mix_input, "fs", axis=0, tiled=True),
        lax.all_gather(mix_branch, "fs", axis=0, tiled=True),
        lax.all_gather(mix_output, "fs", axis=0, tiled=True),
    )
    lane_input = jnp.dot(normed, whole_input, preferred_element_type=jnp.float32).astype(
        jnp.bfloat16
    )
    branch_value = jnp.dot(normed, whole_branch, preferred_element_type=jnp.float32)
    width = lane_input.shape[1]
    lanes = lane_input.reshape(-1, SEQ, width).astype(jnp.float32)
    count = lanes.shape[0]
    padded = jnp.pad(lanes, ((0, 0), (CONV - 1, 0), (0, 0)))
    conv_sum = jnp.zeros_like(lanes)
    for offset in range(CONV):
        conv_sum = conv_sum + padded[:, offset : offset + SEQ] * conv_weight[offset].astype(
            jnp.float32
        )
    conv_out = conv_sum.astype(jnp.bfloat16)
    blocks = conv_out.reshape(count, SEQ, -1, HEAD_DIM)
    rate = jax.nn.sigmoid(
        jnp.einsum("nshd,hde->nshe", blocks, rate_weight, preferred_element_type=jnp.float32)
    ).reshape(lanes.shape)
    admit = jax.nn.sigmoid(
        jnp.einsum("nshd,hde->nshe", blocks, input_weight, preferred_element_type=jnp.float32)
    ).reshape(lanes.shape)
    shift = jnp.repeat(decay_shift.reshape(count, SEQ, -1), HEAD_DIM, axis=-1)
    log_decay = rate_scale * rate * jax.nn.log_sigmoid(decay_param) + shift
    drive = jnp.sqrt(-jnp.expm1(2.0 * log_decay)) * admit * conv_out.astype(jnp.float32)
    _, state = lax.associative_scan(combine_steps, (jnp.exp(log_decay), drive), axis=1)
    mixed_lane = (state.reshape(-1, width) * jax.nn.gelu(branch_value)).astype(jnp.bfloat16)
    total = reduce_back(contract_last(mixed_lane, whole_output))
    return (stream.astype(jnp.float32) + total).astype(jnp.bfloat16)


def shards(
    tokens,
    first_gain,
    first_gate,
    first_up,
    first_down,
    mix_gain,
    mix_input,
    mix_branch,
    conv_weight,
    rate_weight,
    input_weight,
    decay_param,
    decay_shift,
    mix_output,
    second_gain,
    second_gate,
    second_up,
    second_down,
    final_gain,
):
    stream = half_step(tokens, first_gain, first_gate, first_up, first_down)
    stream = lane_mixer(
        stream,
        mix_gain,
        mix_input,
        mix_branch,
        conv_weight,
        rate_weight,
        input_weight,
        decay_param,
        decay_shift,
        mix_output,
    )
    stream = half_step(stream, second_gain, second_gate, second_up, second_down)
    values = stream.astype(jnp.float32)
    squares = lax.psum(jnp.sum(values * values, axis=1), "tp")
    scale = lax.rsqrt(squares / D + norm_eps)
    return (values * scale[:, None] * final_gain).astype(jnp.bfloat16)


def solution(mesh):
    return jax.shard_map(
        shards,
        mesh=mesh,
        in_specs=(
            P("fs", "tp"),
            P(),
            P("fs", "tp"),
            P("fs", "tp"),
            P("fs", "tp"),
            P(),
            P("fs", "tp"),
            P("fs", "tp"),
            P(None, "tp"),
            P("tp", None, None),
            P("tp", None, None),
            P("tp"),
            P("fs", "tp"),
            P("fs", "tp"),
            P(),
            P("fs", "tp"),
            P("fs", "tp"),
            P("fs", "tp"),
            P("tp"),
        ),
        out_specs=P("fs", "tp"),
        check_vma=False,
    )
```

profile of v0, /device:TPU:0, one launch (start us, length us, event | category | flops | bytes accessed | tf_op | source)
XLA Modules:
  0.0 989.3 jit_solution(604671720317064304)
XLA Ops:
  9.4 36.7 %all-gather.13.cloned.1.call-done = bf16[1024,2048]{1,0:T(8,128)(2,1)} async-done(((bf16[1024,512]{1,0:T(8,128)(2,1)}), bf16[1024,2048]{1,0:T(8,128)(2,1)}) %all-gather.13.cloned.1.call-update) | async-done | bytes 4194320 | tf_op jit(solution)/shard_map/all_gather | solution.py:23
  46.1 3.1 fusion
  49.2 85.0 %all-gather.15.cloned.1.call-done = bf16[2048,1280]{1,0:T(8,128)(2,1)} async-done(((bf16[256,1280]{1,0:T(8,128)(2,1)}), bf16[2048,1280]{1,0:T(8,128)(2,1)}) %all-gather.15.cloned.1.call-update) | async-done | bytes 5242896 | tf_op jit(solution)/shard_map/all_gather | solution.py:42
  134.2 10.7 %fusion.24 = f32[1024,1280]{1,0:T(8,128)} fusion(bf16[2048,1280]{1,0:T(8,128)(2,1)} %all-gather.15.cloned.1.call-done, bf16[1024,2048]{1,0:T(8,128)(2,1)} %all-gather.13.cloned.1.call-done, f32[2048]{0:T(1024)S(1)} %copy-done.15, f32[1024]{0:T(1024)S(1)} %add_rsqrt_fusion.3), kind=kOutput, calls=%fused_computation.41 | convolution fusion | flops 5377097728 | bytes 14692352 | tf_op jit(solution)/shard_map/dot_general | solution.py:46
  144.9 75.6 %all-gather.17.cloned.1.call-done = bf16[2048,1280]{1,0:T(8,128)(2,1)} async-done(((bf16[256,1280]{1,0:T(8,128)(2,1)}), bf16[2048,1280]{1,0:T(8,128)(2,1)}) %all-gather.17.cloned.1.call-update) | async-done | bytes 5242896 | tf_op jit(solution)/shard_map/all_gather | solution.py:43
  220.5 86.1 %all-gather.19.cloned.1.call-done = bf16[2048,1280]{1,0:T(8,128)(2,1)} async-done(((bf16[256,1280]{1,0:T(8,128)(2,1)}), bf16[2048,1280]{1,0:T(8,128)(2,1)}) %all-gather.19.cloned.1.call-update) | async-done | bytes 5242896 | tf_op jit(solution)/shard_map/all_gather | solution.py:44
  306.6 19.8 %convolution_convert_fusion.2 = bf16[1024,2048]{1,0:T(8,128)(2,1)} fusion(bf16[2048,1280]{1,0:T(8,128)(2,1)} %all-gather.19.cloned.1.call-done, f32[1024,1280]{1,0:T(8,128)} %fusion.24, bf16[2048,1280]{1,0:T(8,128)(2,1)} %all-gather.17.cloned.1.call-done, bf16[1024,2048]{1,0:T(8,128)(2,1)} %all-gather.13.cloned.1.call-done, f32[2048]{0:T(1024)S(1)} %copy-done.15, ...), kind=kOutput, calls=%fused_computation.19 | convolution fusion | flops 10755768320 | bytes 24129536 | tf_op jit(solution)/shard_map/dot_general | solution.py:34
  326.5 42.7 %reduce-scatter.4.cloned.1.call-done = bf16[1024,512]{1,0:T(8,128)(2,1)} async-done(((bf16[1024,2048]{1,0:T(8,128)(2,1)}), bf16[1024,512]{1,0:T(8,128)(2,1)}) %reduce-scatter.4.cloned.1.call-update) | async-done | bytes 1048592 | tf_op jit(solution)/shard_map/reduce_scatter | solution.py:28
  369.2 2.5 add_convert_fusion.2
  375.7 30.7 %all-gather.21.cloned.1.call-done = bf16[1024,2048]{1,0:T(8,128)(2,1)} async-done(((bf16[1024,512]{1,0:T(8,128)(2,1)}), bf16[1024,2048]{1,0:T(8,128)(2,1)}) %all-gather.21.cloned.1.call-update) | async-done | bytes 4194320 | tf_op jit(solution)/shard_map/all_gather | solution.py:23
  406.4 3.1 fusion.3
  409.5 39.3 %all-gather.23.cloned.1.call-done = bf16[2048,256]{1,0:T(8,128)(2,1)} async-done(((bf16[256,256]{1,0:T(8,128)(2,1)}), bf16[2048,256]{1,0:T(8,128)(2,1)}) %all-gather.23.cloned.1.call-update) | async-done | bytes 1048592 | tf_op jit(solution)/shard_map/all_gather | solution.py:72
  448.8 3.8 convolution_convert_fusion.3
  457.1 2.7 fusion.58
  459.8 2.3 slice.263
  462.1 2.1 slice.264
  464.2 2.1 slice.262
  466.3 2.1 slice.266
  555.9 2.8 pad.85
  559.8 9.3 convolution_convert_fusion.1
  569.3 43.3 %reduce-scatter.6.cloned.1.call-done = bf16[1024,512]{1,0:T(8,128)(2,1)} async-done(((bf16[1024,2048]{1,0:T(8,128)(2,1)}), bf16[1024,512]{1,0:T(8,128)(2,1)}) %reduce-scatter.6.cloned.1.call-update) | async-done | bytes 1048592 | tf_op jit(solution)/shard_map/reduce_scatter | solution.py:28
  612.5 2.5 add_convert_fusion.1
  617.0 32.7 %all-gather.29.cloned.1.call-done = bf16[1024,2048]{1,0:T(8,128)(2,1)} async-done(((bf16[1024,512]{1,0:T(8,128)(2,1)}), bf16[1024,2048]{1,0:T(8,128)(2,1)}) %all-gather.29.cloned.1.call-update) | async-done | bytes 4194320 | tf_op jit(solution)/shard_map/all_gather | solution.py:23
  649.7 3.1 fusion.6
  652.7 84.9 %all-gather.31.cloned.1.call-done = bf16[2048,1280]{1,0:T(8,128)(2,1)} async-done(((bf16[256,1280]{1,0:T(8,128)(2,1)}), bf16[2048,1280]{1,0:T(8,128)(2,1)}) %all-gather.31.cloned.1.call-update) | async-done | bytes 5242896 | tf_op jit(solution)/shard_map/all_gather | solution.py:42
  737.6 10.7 %fusion.19 = f32[1024,1280]{1,0:T(8,128)} fusion(bf16[2048,1280]{1,0:T(8,128)(2,1)} %all-gather.31.cloned.1.call-done, bf16[1024,2048]{1,0:T(8,128)(2,1)} %all-gather.29.cloned.1.call-done, f32[2048]{0:T(1024)S(1)} %copy-done.18, f32[1024]{0:T(1024)S(1)} %add_rsqrt_fusion.1), kind=kOutput, calls=%fused_computation.40 | convolution fusion | flops 5377097728 | bytes 14692352 | tf_op jit(solution)/shard_map/dot_general | solution.py:46
  748.3 75.6 %all-gather.33.cloned.1.call-done = bf16[2048,1280]{1,0:T(8,128)(2,1)} async-done(((bf16[256,1280]{1,0:T(8,128)(2,1)}), bf16[2048,1280]{1,0:T(8,128)(2,1)}) %all-gather.33.cloned.1.call-update) | async-done | bytes 5242896 | tf_op jit(solution)/shard_map/all_gather | solution.py:43
  823.9 86.1 %all-gather.35.cloned.1.call-done = bf16[2048,1280]{1,0:T(8,128)(2,1)} async-done(((bf16[256,1280]{1,0:T(8,128)(2,1)}), bf16[2048,1280]{1,0:T(8,128)(2,1)}) %all-gather.35.cloned.1.call-update) | async-done | bytes 5242896 | tf_op jit(solution)/shard_map/all_gather | solution.py:44
  910.0 19.8 %convolution_convert_fusion = bf16[1024,2048]{1,0:T(8,128)(2,1)} fusion(bf16[2048,1280]{1,0:T(8,128)(2,1)} %all-gather.35.cloned.1.call-done, f32[1024,1280]{1,0:T(8,128)} %fusion.19, bf16[2048,1280]{1,0:T(8,128)(2,1)} %all-gather.33.cloned.1.call-done, bf16[1024,2048]{1,0:T(8,128)(2,1)} %all-gather.29.cloned.1.call-done, f32[2048]{0:T(1024)S(1)} %copy-done.18, ...), kind=kOutput, calls=%fused_computation.17 | convolution fusion | flops 10755768320 | bytes 24129536 | tf_op jit(solution)/shard_map/dot_general | solution.py:34
  929.9 42.8 %reduce-scatter.8.cloned.1.call-done = bf16[1024,512]{1,0:T(8,128)(2,1)} async-done(((bf16[1024,2048]{1,0:T(8,128)(2,1)}), bf16[1024,512]{1,0:T(8,128)(2,1)}) %reduce-scatter.8.cloned.1.call-update) | async-done | bytes 1048592 | tf_op jit(solution)/shard_map/reduce_scatter | solution.py:28
  974.3 5.8 psum.7
  980.1 2.7 fusion.11
  (196 shorter events, 103.3 us)
Async XLA Ops:
  6.5 446.9 %copy-start = (bf16[4,64,64]{2,1,0:T(8,128)(2,1)S(1)}, bf16[4,64,64]{2,1,0:T(8,128)(2,1)}, u32[]{:S(2)}) copy-start(bf16[4,64,64]{2,1,0:T(8,128)(2,1)} %param.28) | copy-start | bytes 98308
  6.5 127.7 %copy-start.15 = (f32[2048]{0:T(1024)S(1)}, f32[2048]{0:T(1024)}, u32[]{:S(2)}) copy-start(f32[2048]{0:T(1024)} %param.20) | copy-start | bytes 24580
  6.5 39.6 %all-gather.13.cloned.1.call-start = ((), (), s32[]{:S(2)}) async-start(), calls=%async_computation.3 | async-start | bytes 5242880 | tf_op jit(solution)/shard_map/all_gather | solution.py:23
  7.3 126.9 %all-gather.15.cloned.1.call-start = ((), (), s32[]{:S(2)}) async-start(), calls=%async_computation.4 | async-start | bytes 5898240 | tf_op jit(solution)/shard_map/all_gather | solution.py:42
  8.0 212.5 %all-gather.17.cloned.1.call-start = ((), (), s32[]{:S(2)}) async-start(), calls=%async_computation.5 | async-start | bytes 5898240 | tf_op jit(solution)/shard_map/all_gather | solution.py:43
  8.7 297.9 %all-gather.19.cloned.1.call-start = ((), (), s32[]{:S(2)}) async-start(), calls=%async_computation.6 | async-start | bytes 5898240 | tf_op jit(solution)/shard_map/all_gather | solution.py:44
  9.3 359.9 %reduce-scatter.4.cloned.1.call-start = ((), (), s32[]{:S(2)}) async-start(), calls=%async_computation.7 | async-start | bytes 5242880 | tf_op jit(solution)/shard_map/reduce_scatter | solution.py:28
  144.9 224.3 %copy-start.4 = (bf16[1024,512]{1,0:T(8,128)(2,1)S(1)}, bf16[1024,512]{1,0:T(8,128)(2,1)}, u32[]{:S(2)}) copy-start(bf16[1024,512]{1,0:T(8,128)(2,1)} %param.19) | copy-start | bytes 3145732
  326.4 47.8 %copy-start.7 = (bf16[4,256]{1,0:T(4,128)(2,1)S(1)}, bf16[4,256]{1,0:T(4,128)(2,1)}, u32[]{:S(2)}) copy-start(bf16[4,256]{1,0:T(4,128)(2,1)} %param.27) | copy-start | bytes 6148
  326.4 47.8 %copy-start.6 = (f32[1024,4]{0,1:T(4,128)S(1)}, f32[1024,4]{0,1:T(4,128)}, u32[]{:S(2)}) copy-start(f32[1024,4]{0,1:T(4,128)} %param.31) | copy-start | bytes 49156
  326.4 49.3 %copy-start.13 = (f32[256]{0:T(256)S(1)}, f32[256]{0:T(256)}, u32[]{:S(2)}) copy-start(f32[256]{0:T(256)} %param.30) | copy-start | bytes 3076
  326.4 122.4 %copy-start.16 = (f32[2048]{0:T(1024)S(1)}, f32[2048]{0:T(1024)}, u32[]{:S(2)}) copy-start(f32[2048]{0:T(1024)} %param.24) | copy-start | bytes 24580
  326.5 79.9 %all-gather.21.cloned.1.call-start = ((), (), s32[]{:S(2)}) async-start(), calls=%async_computation.8 | async-start | bytes 5242880 | tf_op jit(solution)/shard_map/all_gather | solution.py:23
  371.8 77.0 %all-gather.23.cloned.1.call-start = ((), (), s32[]{:S(2)}) async-start(), calls=%async_computation.9 | async-start | bytes 1179648 | tf_op jit(solution)/shard_map/all_gather | solution.py:72
  372.5 186.5 %all-gather.25.cloned.1.call-start = ((), (), s32[]{:S(2)}) async-start(), calls=%async_computation.10 | async-start | bytes 1179648 | tf_op jit(solution)/shard_map/all_gather | solution.py:73
  373.3 185.8 %all-gather.27.cloned.1.call-start = ((), (), s32[]{:S(2)}) async-start(), calls=%async_computation.11 | async-start | bytes 1179648 | tf_op jit(solution)/shard_map/all_gather | solution.py:74
  374.0 238.5 %reduce-scatter.6.cloned.1.call-start = ((), (), s32[]{:S(2)}) async-start(), calls=%async_computation.12 | async-start | bytes 5242880 | tf_op jit(solution)/shard_map/reduce_scatter | solution.py:28
  409.5 43.1 %copy-start.10 = (f32[1024]{0:T(1024)}, f32[1024]{0:T(1024)S(1)}, u32[]{:S(2)}) copy-start(f32[1024]{0:T(1024)S(1)} %add_rsqrt_fusion.2) | copy-start | bytes 12292
  543.6 12.0 %copy-start.9 = (f32[1,1,256]{2,1,0:T(1,128)S(1)}, f32[1,1,256]{2,1,0:T(1,128)}, u32[]{:S(2)}) copy-start(f32[1,1,256]{2,1,0:T(1,128)} %slice.336) | copy-start | bytes 3076
  554.4 4.3 copy-start.8
  555.6 3.5 copy-start.11
  555.6 3.5 copy-start.17
  559.0 53.6 %copy-start.3 = (bf16[1024,512]{1,0:T(8,128)(2,1)S(1)}, bf16[1024,512]{1,0:T(8,128)(2,1)}, u32[]{:S(2)}) copy-start(bf16[1024,512]{1,0:T(8,128)(2,1)} %add_convert_fusion.2) | copy-start | bytes 3145732
  569.2 168.4 %copy-start.18 = (f32[2048]{0:T(1024)S(1)}, f32[2048]{0:T(1024)}, u32[]{:S(2)}) copy-start(f32[2048]{0:T(1024)} %param.33) | copy-start | bytes 24580
  569.2 80.4 %all-gather.29.cloned.1.call-start = ((), (), s32[]{:S(2)}) async-start(), calls=%async_computation.13 | async-start | bytes 5242880 | tf_op jit(solution)/shard_map/all_gather | solution.py:23
  615.0 122.6 %all-gather.31.cloned.1.call-start = ((), (), s32[]{:S(2)}) async-start(), calls=%async_computation.14 | async-start | bytes 5898240 | tf_op jit(solution)/shard_map/all_gather | solution.py:42
  615.6 208.3 %all-gather.33.cloned.1.call-start = ((), (), s32[]{:S(2)}) async-start(), calls=%async_computation.15 | async-start | bytes 5898240 | tf_op jit(solution)/shard_map/all_gather | solution.py:43
  616.4 293.7 %all-gather.35.cloned.1.call-start = ((), (), s32[]{:S(2)}) async-start(), calls=%async_computation.16 | async-start | bytes 5898240 | tf_op jit(solution)/shard_map/all_gather | solution.py:44
  616.9 355.7 %reduce-scatter.8.cloned.1.call-start = ((), (), s32[]{:S(2)}) async-start(), calls=%async_computation.17 | async-start | bytes 5242880 | tf_op jit(solution)/shard_map/reduce_scatter | solution.py:28
  748.3 224.3 %copy-start.2 = (bf16[1024,512]{1,0:T(8,128)(2,1)S(1)}, bf16[1024,512]{1,0:T(8,128)(2,1)}, u32[]{:S(2)}) copy-start(bf16[1024,512]{1,0:T(8,128)(2,1)} %add_convert_fusion.1) | copy-start | bytes 3145732
  910.0 72.8 %copy-start.1 = (bf16[4,64,64]{2,1,0:T(8,128)(2,1)S(1)}, bf16[4,64,64]{2,1,0:T(8,128)(2,1)}, u32[]{:S(2)}) copy-start(bf16[4,64,64]{2,1,0:T(8,128)(2,1)} %param.28) | copy-start | bytes 98308
  929.9 50.3 %copy-start.12 = (f32[512]{0:T(512)S(1)}, f32[512]{0:T(512)}, u32[]{:S(2)}) copy-start(f32[512]{0:T(512)} %param.37) | copy-start | bytes 6148
  (2 other events, 3.8 us)
Sparse Core Ops, SparseCore 0:
  8.9 37.1 all-gather.12
  48.3 85.8 all-gather.14
  136.4 84.0 all-gather.16
  222.5 84.0 all-gather.18
  326.6 42.6 reduce-scatter.3
  371.9 34.4 all-gather.20
  408.5 40.2 all-gather.22
  450.9 38.9 all-gather.24
  492.1 38.9 all-gather.26
  569.3 43.1 reduce-scatter.5
  615.2 34.4 all-gather.28
  651.7 85.8 all-gather.30
  739.8 84.0 all-gather.32
  825.9 84.0 all-gather.34
  930.0 42.5 reduce-scatter.7
where the time goes:
time: 992 us; the launch traced here: 989 us
  waiting for transfers between devices  768 us (77%)
  local copies, waits for them, and re-layouts  78.1 us (8%)
  matrix products  75.1 us (8%)
  other arithmetic  47.8 us (5%)
  between operations  13.8 us (1%)
    all_gather x2, waiting for transfers between devices, half_step(): lax.all_gather(weight_down, 'fs', axis=0, tiled=True)  172 us
    all_gather x2, waiting for transfers between devices, half_step(): lax.all_gather(weight_gate, 'fs', axis=0, tiled=True)  170 us
    all_gather x2, waiting for transfers between devices, half_step(): lax.all_gather(weight_up, 'fs', axis=0, tiled=True)  151 us
    reduce_scatter x3, waiting for transfers between devices, reduce_back(): lax.psum_scatter(partial_value.astype(jnp.bfloat16), 'tp', scatter_dimens...  129 us
    all_gather x3, waiting for transfers between devices, full_rows(): whole = lax.all_gather(stream, 'tp', axis=1, tiled=True)  100 us
    slice x60, local copies, waits for them, and re-layouts, lane_mixer(): lax.associative_scan(combine_steps, (jnp.exp(log_decay), drive), axis=1)  69.1 us
    dot_general x3, matrix products, contract_last(): lax.dot_general(left, right, (((1,), (1,)), ((), ())), preferred_element_...  48.9 us
    all_gather x1, waiting for transfers between devices, lane_mixer(): lax.all_gather(mix_input, 'fs', axis=0, tiled=True)  39.3 us
  transfers between devices with their start and end apart: 15, of which 13 were waited for; matrix products, arithmetic and copies ran while one was open for 14% of the time, Pallas kernels for 0%

commit v1 on v0

--- a/solution.py
+++ b/solution.py
@@ -1,7 +1,10 @@
 import jax
 import jax.numpy as jnp
 from jax import lax
+from jax.experimental import pallas as pl
+from jax.experimental.pallas import tpu as pltpu
 from jax.sharding import PartitionSpec as P
+
 
 D = 2048
 HEAD_DIM = 64
@@ -19,15 +22,84 @@
     return (values * scale * gain).astype(jnp.bfloat16)
 
 
+def after(value, *earlier):
+    return lax.optimization_barrier((value, *earlier))[0]
+
+
+def put(whole, block, row):
+    return lax.dynamic_update_slice(whole, block, (row, jnp.int32(0)))
+
+
+def ring_gather(block):
+    n = lax.axis_size("fs")
+    rows, columns = block.shape
+    order = list(range(0, n, 2)) + list(range(1, n, 2))[::-1]
+    forward = [(order[i], order[(i + 1) % n]) for i in range(n)]
+    backward = [(to, source) for source, to in forward]
+    place = [order.index(i) for i in range(n)]
+    me = lax.axis_index("fs")
+    at = jnp.array(place, jnp.int32)[me]
+    owners = jnp.array(order, jnp.int32)
+    whole = put(jnp.zeros((n * rows, columns), block.dtype), block, me * rows)
+    ahead, back = block, block
+    for step in range(1, (n + 1) // 2):
+        ahead = lax.ppermute(ahead, "fs", forward)
+        back = lax.ppermute(back, "fs", backward)
+        whole = put(whole, ahead, owners[(at - step) % n] * rows)
+        whole = put(whole, back, owners[(at + step) % n] * rows)
+    if n % 2 == 0:
+        half = rows // 2
+        base = owners[(at + n // 2) % n] * rows
+        ahead = lax.ppermute(ahead[:half], "fs", forward)
+        back = lax.ppermute(back[half:], "fs", backward)
+        whole = put(whole, ahead, base)
+        whole = put(whole, back, base + half)
+    return whole, (ahead, back)
+
+
+def tp_maps():
+    n = lax.axis_size("tp")
+    chips = n // 2
+    partner = [(i, i ^ 1) for i in range(n)]
+    hops = [[(i, (i + 2 * d) % n) for i in range(n)] for d in range(1, chips)]
+    return n, chips, partner, hops
+
+
 def full_rows(stream, gain):
-    whole = lax.all_gather(stream, "tp", axis=1, tiled=True)
+    n, chips, partner, hops = tp_maps()
+    me = lax.axis_index("tp")
+    width = stream.shape[1]
+    far = [lax.ppermute(stream, "tp", hop) for hop in hops]
+    whole = jnp.zeros((stream.shape[0], n * width), stream.dtype)
+    blocks = [(stream, 0)] + [(far[d - 1], 2 * d) for d in range(1, chips)]
+    for block, back in blocks:
+        owner = (me - back) % n
+        near = lax.ppermute(block, "tp", partner)
+        whole = lax.dynamic_update_slice(whole, block, (jnp.int32(0), owner * width))
+        whole = lax.dynamic_update_slice(whole, near, (jnp.int32(0), (owner ^ 1) * width))
     return rms_rows(whole, gain)
 
 
 def reduce_back(partial_value):
-    return lax.psum_scatter(
-        partial_value.astype(jnp.bfloat16), "tp", scatter_dimension=1, tiled=True
-    ).astype(jnp.float32)
+    n, chips, partner, hops = tp_maps()
+    me = lax.axis_index("tp")
+    width = partial_value.shape[1] // n
+
+    def block(owner):
+        return lax.dynamic_slice_in_dim(partial_value, owner * width, width, axis=1)
+
+    sums = []
+    for d in list(range(1, chips)) + [0]:
+        owner = (me + 2 * d) % n
+        sent = block(owner ^ 1)
+        near = lax.ppermute(sent, "tp", partner)
+        sums.append(block(owner).astype(jnp.float32) + near.astype(jnp.float32))
+    total = sums[-1]
+    for d in range(1, chips):
+        sent = sums[d - 1].astype(jnp.bfloat16)
+        arrived = lax.ppermute(sent, "tp", hops[d - 1])
+        total = total + arrived.astype(jnp.float32)
+    return total
 
 
 def contract_last(left, right):
@@ -36,43 +108,60 @@
     )
 
 
-def half_step(stream, gain, weight_gate, weight_up, weight_down):
+def half_step(stream, gain, whole_gate, whole_up, whole_down):
     normed = full_rows(stream, gain)
-    whole_gate, whole_up, whole_down = (
-        lax.all_gather(weight_gate, "fs", axis=0, tiled=True),
-        lax.all_gather(weight_up, "fs", axis=0, tiled=True),
-        lax.all_gather(weight_down, "fs", axis=0, tiled=True),
-    )
     gate_value = jnp.dot(normed, whole_gate, preferred_element_type=jnp.float32)
     up_value = jnp.dot(normed, whole_up, preferred_element_type=jnp.float32)
     hidden = (jax.nn.silu(gate_value) * up_value).astype(jnp.bfloat16)
-    partial_value = contract_last(hidden, whole_down)
+    partial_value = contract_last(hidden, whole_down).astype(jnp.bfloat16)
     total = reduce_back(partial_value)
     return (stream.astype(jnp.float32) + 0.5 * total).astype(jnp.bfloat16)
 
 
-def combine_steps(earlier, later):
-    return (earlier[0] * later[0], later[0] * earlier[1] + later[1])
+def scan_kernel(decay_ref, drive_ref, state_ref):
+    decay, drive = decay_ref[...], drive_ref[...]
+    rows = decay.shape[0]
+    row = lax.broadcasted_iota(jnp.int32, decay.shape, 0)
+    shift = 1
+    while shift < rows:
+        inside = row >= shift
+        before_decay = jnp.where(inside, pltpu.roll(decay, shift, 0), 1.0)
+        before_drive = jnp.where(inside, pltpu.roll(drive, shift, 0), 0.0)
+        drive = decay * before_drive + drive
+        decay = decay * before_decay
+        shift *= 2
+    state_ref[...] = drive
+
+
+def scan_states(decay, drive):
+    rows, width = decay.shape
+    lanes = min(width, 128)
+    spec = pl.BlockSpec((SEQ, lanes), lambda i, j: (i, j))
+    return pl.pallas_call(
+        scan_kernel,
+        grid=(rows // SEQ, width // lanes),
+        in_specs=[spec, spec],
+        out_specs=spec,
+        out_shape=jax.ShapeDtypeStruct((rows, width), jnp.float32),
+        cost_estimate=pl.CostEstimate(
+            flops=rows * width * 60, bytes_accessed=rows * width * 12, transcendentals=0
+        ),
+    )(decay, drive)
 
 
 def lane_mixer(
     stream,
     gain,
-    mix_input,
-    mix_branch,
+    whole_input,
+    whole_branch,
     conv_weight,
     rate_weight,
     input_weight,
     decay_param,
     decay_shift,
-    mix_output,
+    whole_output,
 ):
     normed = full_rows(stream, gain)
-    whole_input, whole_branch, whole_output = (
-        lax.all_gather(mix_input, "fs", axis=0, tiled=True),
-        lax.all_gather(mix_branch, "fs", axis=0, tiled=True),
-        lax.all_gather(mix_output, "fs", axis=0, tiled=True),
-    )
     lane_input = jnp.dot(normed, whole_input, preferred_element_type=jnp.float32).astype(
         jnp.bfloat16
     )
@@ -97,9 +186,10 @@
     shift = jnp.repeat(decay_shift.reshape(count, SEQ, -1), HEAD_DIM, axis=-1)
     log_decay = rate_scale * rate * jax.nn.log_sigmoid(decay_param) + shift
     drive = jnp.sqrt(-jnp.expm1(2.0 * log_decay)) * admit * conv_out.astype(jnp.float32)
-    _, state = lax.associative_scan(combine_steps, (jnp.exp(log_decay), drive), axis=1)
-    mixed_lane = (state.reshape(-1, width) * jax.nn.gelu(branch_value)).astype(jnp.bfloat16)
-    total = reduce_back(contract_last(mixed_lane, whole_output))
+    state = scan_states(jnp.exp(log_decay).reshape(-1, width), drive.reshape(-1, width))
+    mixed_lane = (state * jax.nn.gelu(branch_value)).astype(jnp.bfloat16)
+    partial_value = contract_last(mixed_lane, whole_output).astype(jnp.bfloat16)
+    total = reduce_back(partial_value)
     return (stream.astype(jnp.float32) + total).astype(jnp.bfloat16)
 
 
@@ -124,20 +214,28 @@
     second_down,
     final_gain,
 ):
-    stream = half_step(tokens, first_gain, first_gate, first_up, first_down)
+    lanes = mix_input.shape[1]
+    units = first_down.shape[1]
+    first, done = ring_gather(jnp.concatenate([first_gate, first_up], axis=1))
+    down, done = ring_gather(after(first_down, *done))
+    rest = jnp.concatenate([mix_input, mix_branch, mix_output, second_gate], axis=1)
+    rest, done = ring_gather(after(rest, *done))
+    last = jnp.concatenate([second_up, second_down], axis=1)
+    last, done = ring_gather(after(last, *done))
+    stream = half_step(tokens, first_gain, first[:, :units], first[:, units:], down)
     stream = lane_mixer(
         stream,
         mix_gain,
-        mix_input,
-        mix_branch,
+        rest[:, :lanes],
+        rest[:, lanes : 2 * lanes],
         conv_weight,
         rate_weight,
         input_weight,
         decay_param,
         decay_shift,
-        mix_output,
-    )
-    stream = half_step(stream, second_gain, second_gate, second_up, second_down)
+        rest[:, 2 * lanes : 3 * lanes],
+    )
+    stream = half_step(stream, second_gain, rest[:, 3 * lanes :], last[:, :units], last[:, units:])
     values = stream.astype(jnp.float32)
     squares = lax.psum(jnp.sum(values * values, axis=1), "tp")
     scale = lax.rsqrt(squares / D + norm_eps)

time: 992 us -> 504 us (0.51)
  waiting for transfers between devices: 768 us -> 248 us
  starting transfers between devices: 0.73 us -> 45.8 us
  other arithmetic: 47.8 us -> 27.9 us
    all_gather x12 -> x0, waiting for transfers between devices: 633 us -> none  [the longest x2 172 us: half_step(): lax.all_gather(weight_down, 'fs', axis=0, tiled=True)]
    ppermute x0 -> x50, waiting for transfers between devices: none -> 248 us  [the longest x12 165 us: ring_gather(): ahead = lax.ppermute(ahead, 'fs', forward)]
    reduce_scatter x3 -> x0, waiting for transfers between devices: 129 us -> none  [reduce_back(): lax.psum_scatter(partial_value.astype(jnp.bfloat16), 'tp', scatter_dimens...]
    slice x60 -> x8, local copies, waits for them, and re-layouts: 69.1 us -> 0.3 us  [the longest x4 0.15 us: ring_gather(): back = lax.ppermute(back[half:], 'fs', backward)]
    ppermute x0 -> x50, starting transfers between devices: none -> 45.8 us  [the longest x12 22.7 us: ring_gather(): ahead = lax.ppermute(ahead, 'fs', forward)]
    dynamic_update_slice x0 -> x46, local copies, waits for them, and re-layouts: none -> 42.8 us  [the longest x36 33.7 us: put(): return lax.dynamic_update_slice(whole, block, (row, jnp.int32(0)))]
    dot_general x2 -> x1, matrix products: 21.4 us -> 7.61 us  [half_step(): gate_value = jnp.dot(normed, whole_gate, preferred_element_type=jnp.float32)]
    mul x8 -> x0, other arithmetic: 11.8 us -> none  [combine_steps(): return (earlier[0] * later[0], later[0] * earlier[1] + later[1])]
  transfers between devices with their start and end apart: 15 -> 50, of which waited for: 13 -> 24; matrix products, arithmetic and copies ran while one was open for 14% -> 17% of each run, Pallas kernels for 0% -> 0%
where the time goes in v1:
time: 504 us; the launch traced here: 496 us
  waiting for transfers between devices  248 us (49%)
  local copies, waits for them, and re-layouts  83.3 us (17%)
  matrix products  71.1 us (14%)
  starting transfers between devices  45.8 us (9%)
  other arithmetic  27.9 us (6%)
  between operations  10.2 us (2%)
  blocking collectives  6.04 us (1%)
    ppermute x12, waiting for transfers between devices, ring_gather(): ahead = lax.ppermute(ahead, 'fs', forward)  165 us
    dot_general x3, matrix products, contract_last(): lax.dot_general(left, right, (((1,), (1,)), ((), ())), preferred_element_...  49.5 us
    dynamic_update_slice x36, local copies, waits for them, and re-layouts, put(): return lax.dynamic_update_slice(whole, block, (row, jnp.int32(0)))  33.7 us
    ppermute x4, waiting for transfers between devices, ring_gather(): ahead = lax.ppermute(ahead[:half], 'fs', forward)  33.7 us
    ppermute x3, waiting for transfers between devices, reduce_back(): arrived = lax.ppermute(sent, 'tp', hops[d - 1])  24.4 us
    ppermute x12, starting transfers between devices, ring_gather(): ahead = lax.ppermute(ahead, 'fs', forward)  22.7 us
    ppermute x3, waiting for transfers between devices, full_rows(): far = [lax.ppermute(stream, 'tp', hop) for hop in hops]  17.1 us
    dot_general x1, matrix products, half_step(): up_value = jnp.dot(normed, whole_up, preferred_element_type=jnp.float32)  10.7 us
  transfers between devices with their start and end apart: 50, of which 24 were waited for; matrix products, arithmetic and copies ran while one was open for 17% of the time, Pallas kernels for 0%

profile of v1, /device:TPU:0, one launch (start us, length us, event | category | flops | bytes accessed | tf_op | source)
XLA Modules:
  0.0 496.3 jit_solution(12852514795648863794)
XLA Ops:
  2.3 3.1 collective-permute-start.3
  7.4 4.7 broadcast.158.clone.1
  13.3 17.1 %collective-permute-done.1 = bf16[1024,512]{1,0:T(8,128)(2,1)} collective-permute-done((bf16[1024,512]{1,0:T(8,128)(2,1)}, bf16[1024,512]{1,0:T(8,128)(2,1)}, u32[]{:S(2)}, u32[]{:S(2)}) %collective-permute-start.1) | collective-permute-done | bytes 1048608 | tf_op jit(solution)/shard_map/ppermute | solution.py:72
  30.4 3.9 collective-permute-done.3
  66.5 3.1 fusion
  73.2 20.5 %collective-permute-done.7 = bf16[256,2560]{1,0:T(8,128)(2,1)S(1)} collective-permute-done((bf16[256,2560]{1,0:T(8,128)(2,1)}, bf16[256,2560]{1,0:T(8,128)(2,1)S(1)}, u32[]{:S(2)}, u32[]{:S(2)}) %collective-permute-start.7) | collective-permute-done | bytes 1310752 | tf_op jit(solution)/shard_map/ppermute | solution.py:46
  98.4 10.1 %collective-permute-done.9 = bf16[128,2560]{1,0:T(8,128)(2,1)S(1)} collective-permute-done((bf16[128,2560]{1,0:T(8,128)(2,1)S(1)}, bf16[128,2560]{1,0:T(8,128)(2,1)S(1)}, u32[]{:S(2)}, u32[]{:S(2)}) %collective-permute-start.9) | collective-permute-done | bytes 655392 | tf_op jit(solution)/shard_map/ppermute | solution.py:53
  112.7 11.1 %collective-permute-done.11 = bf16[256,1280]{1,0:T(8,128)(2,1)S(1)} collective-permute-done((bf16[256,1280]{1,0:T(8,128)(2,1)S(1)}, bf16[256,1280]{1,0:T(8,128)(2,1)S(1)}, u32[]{:S(2)}, u32[]{:S(2)}) %collective-permute-start.11) | collective-permute-done | bytes 655392 | tf_op jit(solution)/shard_map/ppermute | solution.py:46
  125.8 10.7 %fusion.15 = f32[1024,1280]{1,0:T(8,128)} fusion(bf16[2048,2560]{1,0:T(8,128)(2,1)} %constant_dynamic-update-slice_fusion.35, bf16[1024,2048]{1,0:T(8,128)(2,1)} %constant_dynamic-update-slice_fusion.44, f32[2048]{0:T(1024)S(1)} %copy-done.23, f32[1024]{0:T(1024)S(1)} %add_rsqrt_fusion.3), kind=kOutput, calls=%fused_computation.21 | convolution fusion | flops 5377097728 | bytes 14692352 | tf_op jit(solution)/shard_map/dot_general | solution.py:114
  136.5 2.6 broadcast_in_dim.10
  145.6 9.4 %collective-permute-done.15 = bf16[256,1280]{1,0:T(8,128)(2,1)S(1)} collective-permute-done((bf16[256,1280]{1,0:T(8,128)(2,1)S(1)}, bf16[256,1280]{1,0:T(8,128)(2,1)S(1)}, u32[]{:S(2)}, u32[]{:S(2)}) %collective-permute-start.15) | collective-permute-done | bytes 655392 | tf_op jit(solution)/shard_map/ppermute | solution.py:46
  159.4 2.7 collective-permute-done.17
  165.1 20.0 %convolution_convert_fusion.1 = bf16[1024,2048]{1,0:T(8,128)(2,1)} fusion(bf16[2048,1280]{1,0:T(8,128)(2,1)} %constant_dynamic-update-slice_fusion, f32[1024,1280]{1,0:T(8,128)} %fusion.15, bf16[2048,2560]{1,0:T(8,128)(2,1)} %constant_dynamic-update-slice_fusion.35, bf16[1024,2048]{1,0:T(8,128)(2,1)} %constant_dynamic-update-slice_fusion.44, ...), kind=kOutput, calls=%fused_computation.29 | convolution fusion | flops 10755768320 | bytes 24129536 | tf_op jit(solution)/shard_map/dot_general | solution.py:106
  185.1 3.0 constant_dynamic-slice_fusion
  191.2 2.9 add_convert_fusion.5
  195.6 18.5 %collective-permute-done.25 = bf16[256,2048]{1,0:T(8,128)(2,1)} collective-permute-done((bf16[256,2048]{1,0:T(8,128)(2,1)S(1)}, bf16[256,2048]{1,0:T(8,128)(2,1)}, u32[]{:S(2)}, u32[]{:S(2)}) %collective-permute-start.25) | collective-permute-done | bytes 1048608 | tf_op jit(solution)/shard_map/ppermute | solution.py:46
  224.2 14.9 %collective-permute-done.27 = bf16[256,2048]{1,0:T(8,128)(2,1)} collective-permute-done((bf16[256,2048]{1,0:T(8,128)(2,1)}, bf16[256,2048]{1,0:T(8,128)(2,1)}, u32[]{:S(2)}, u32[]{:S(2)}) %collective-permute-start.27) | collective-permute-done | bytes 1048608 | tf_op jit(solution)/shard_map/ppermute | solution.py:46
  247.7 15.4 %collective-permute-done.29 = bf16[256,2048]{1,0:T(8,128)(2,1)S(1)} collective-permute-done((bf16[256,2048]{1,0:T(8,128)(2,1)}, bf16[256,2048]{1,0:T(8,128)(2,1)S(1)}, u32[]{:S(2)}, u32[]{:S(2)}) %collective-permute-start.29) | collective-permute-done | bytes 1048608 | tf_op jit(solution)/shard_map/ppermute | solution.py:46
  266.3 8.7 %collective-permute-done.31 = bf16[128,2048]{1,0:T(8,128)(2,1)S(1)} collective-permute-done((bf16[128,2048]{1,0:T(8,128)(2,1)S(1)}, bf16[128,2048]{1,0:T(8,128)(2,1)S(1)}, u32[]{:S(2)}, u32[]{:S(2)}) %collective-permute-start.31) | collective-permute-done | bytes 524320 | tf_op jit(solution)/shard_map/ppermute | solution.py:53
  292.1 2.7 add_exponential_fusion.decay_ref
  294.7 3.3 multiply_bitcast_fusion.drive_ref
  298.0 3.5 shard_map.253
  301.5 9.7 %convolution_convert_fusion = bf16[1024,2048]{1,0:T(8,128)(2,1)} fusion(f32[1024,256]{1,0:T(8,128)} %shard_map.253, bf16[1024,2048]{1,0:T(8,128)(2,1)} %copy-done.3, f32[2048]{0:T(1024)S(1)} %copy-done.24, f32[1024]{0:T(1024)S(1)} %add_rsqrt_fusion.2, bf16[2048,2048]{1,0:T(8,128)(2,1)} %copy-done.5), kind=kOutput, calls=%fused_computation.28 | convolution fusion | flops 2160590848 | bytes 11546624 | tf_op jit(solution)/shard_map/dot_general | solution.py:106
  320.4 25.1 %collective-permute-done.39 = bf16[256,2560]{1,0:T(8,128)(2,1)} collective-permute-done((bf16[256,2560]{1,0:T(8,128)(2,1)S(1)}, bf16[256,2560]{1,0:T(8,128)(2,1)}, u32[]{:S(2)}, u32[]{:S(2)}) %collective-permute-start.39) | collective-permute-done | bytes 1310752 | tf_op jit(solution)/shard_map/ppermute | solution.py:46
  354.4 21.7 %collective-permute-done.41 = bf16[256,2560]{1,0:T(8,128)(2,1)} collective-permute-done((bf16[256,2560]{1,0:T(8,128)(2,1)}, bf16[256,2560]{1,0:T(8,128)(2,1)}, u32[]{:S(2)}, u32[]{:S(2)}) %collective-permute-start.41) | collective-permute-done | bytes 1310752 | tf_op jit(solution)/shard_map/ppermute | solution.py:46
  382.9 22.8 %collective-permute-done.43 = bf16[256,2560]{1,0:T(8,128)(2,1)S(1)} collective-permute-done((bf16[256,2560]{1,0:T(8,128)(2,1)}, bf16[256,2560]{1,0:T(8,128)(2,1)S(1)}, u32[]{:S(2)}, u32[]{:S(2)}) %collective-permute-start.43) | collective-permute-done | bytes 1310752 | tf_op jit(solution)/shard_map/ppermute | solution.py:46
  408.3 12.1 %collective-permute-done.45 = bf16[128,2560]{1,0:T(8,128)(2,1)S(1)} collective-permute-done((bf16[128,2560]{1,0:T(8,128)(2,1)S(1)}, bf16[128,2560]{1,0:T(8,128)(2,1)S(1)}, u32[]{:S(2)}, u32[]{:S(2)}) %collective-permute-start.45) | collective-permute-done | bytes 655392 | tf_op jit(solution)/shard_map/ppermute | solution.py:53
  422.2 3.8 copy-done.4
  428.1 7.6 %fusion.13 = f32[1024,1280]{1,0:T(8,128)} fusion(bf16[2048,2048]{1,0:T(8,128)(2,1)S(1)} %bitcast.55, bf16[1024,2048]{1,0:T(8,128)(2,1)S(1)} %constant_dynamic-update-slice_fusion.5, f32[2048]{0:T(1024)S(1)} %copy-done.25, f32[1024]{0:T(1024)S(1)} %add_rsqrt_fusion.1), kind=kOutput, calls=%fused_computation.19 | convolution fusion | flops 5377097728 | bytes 14692352 | tf_op jit(solution)/shard_map/dot_general | solution.py:113
  435.7 19.8 %fusion.19 = bf16[1024,2048]{1,0:T(8,128)(2,1)} fusion(bf16[2048,2560]{1,0:T(8,128)(2,1)} %copy-done.4, f32[1024,1280]{1,0:T(8,128)} %fusion.13, bf16[1024,2048]{1,0:T(8,128)(2,1)} %copy-done.2, f32[2048]{0:T(1024)S(1)} %copy-done.25, f32[1024]{0:T(1024)S(1)} %add_rsqrt_fusion.1), kind=kOutput, calls=%fused_computation.27 | convolution fusion | flops 10755768320 | bytes 24129536 | tf_op jit(solution)/shard_map/dot_general | solution.py:106
  463.0 23.7 %collective-permute-done.49 = bf16[1024,512]{1,0:T(8,128)(2,1)S(1)} collective-permute-done((bf16[1024,512]{1,0:T(8,128)(2,1)S(1)}, bf16[1024,512]{1,0:T(8,128)(2,1)S(1)}, u32[]{:S(2)}, u32[]{:S(2)}) %collective-permute-start.49) | collective-permute-done | bytes 1048608 | tf_op jit(solution)/shard_map/ppermute | solution.py:100
  488.7 6.0 %psum.7 = f32[1024]{0:T(1024)S(1)} all-reduce(f32[1024]{0:T(1024)S(1)} %get-tuple-element.11), channel_id=1, replica_groups=mesh['fs'=8,'tp'=4] {'tp'}, use_global_device_ids=true, to_apply=%region_4.5 | all-reduce | flops 1024 | bytes 8192 | tf_op jit(solution)/shard_map/psum | solution.py:240
  (234 shorter events, 141.9 us)
Async XLA Ops:
  2.3 31.9 %collective-permute-start.3 = (bf16[256,2560]{1,0:T(8,128)(2,1)S(1)}, bf16[256,2560]{1,0:T(8,128)(2,1)}, u32[]{:S(2)}, u32[]{:S(2)}) collective-permute-start(bf16[256,2560]{1,0:T(8,128)(2,1)S(1)} %constant_dynamic-update-slice_fusion.48), channel_id=1, source_target_pairs={{0,8},{8,16},{16,24},{24,28},{28,20},{20,12},{12,4},{4,0},{1,9},{9... | collective-permute-start | bytes 3932168 | tf_op jit(solution)/shard_map/ppermute | solution.py:46
  5.4 30.6 %collective-permute-start.4 = (bf16[256,2560]{1,0:T(8,128)(2,1)S(1)}, bf16[256,2560]{1,0:T(8,128)(2,1)}, u32[]{:S(2)}, u32[]{:S(2)}) collective-permute-start(bf16[256,2560]{1,0:T(8,128)(2,1)S(1)} %constant_dynamic-update-slice_fusion.48), channel_id=1, source_target_pairs={{8,0},{16,8},{24,16},{28,24},{20,28},{12,20},{4,12},{0,4},{9,1},{1... | collective-permute-start | bytes 3932168 | tf_op jit(solution)/shard_map/ppermute | solution.py:47
  5.4 24.9 %collective-permute-start.1 = (bf16[1024,512]{1,0:T(8,128)(2,1)}, bf16[1024,512]{1,0:T(8,128)(2,1)}, u32[]{:S(2)}, u32[]{:S(2)}) collective-permute-start(bf16[1024,512]{1,0:T(8,128)(2,1)} %param.27), channel_id=1, source_target_pairs={{0,2},{1,3},{2,0},{3,1},{4,6},{5,7},{6,4},{7,5},{8,10},{9,11},{10,... | collective-permute-start | bytes 3145736 | tf_op jit(solution)/shard_map/ppermute | solution.py:72
  7.4 43.1 %collective-permute-start = (bf16[1024,512]{1,0:T(8,128)(2,1)}, bf16[1024,512]{1,0:T(8,128)(2,1)}, u32[]{:S(2)}, u32[]{:S(2)}) collective-permute-start(bf16[1024,512]{1,0:T(8,128)(2,1)} %param.27), channel_id=1, source_target_pairs={{0,1},{1,0},{2,3},{3,2},{4,5},{5,4},{6,7},{7,6},{8,9},{9,8},{10,11... | collective-permute-start | bytes 3145736 | tf_op jit(solution)/shard_map/ppermute | solution.py:77
  30.3 29.7 %collective-permute-start.2 = (bf16[1024,512]{1,0:T(8,128)(2,1)}, bf16[1024,512]{1,0:T(8,128)(2,1)}, u32[]{:S(2)}, u32[]{:S(2)}) collective-permute-start(bf16[1024,512]{1,0:T(8,128)(2,1)} %collective-permute-done.1), channel_id=1, source_target_pairs={{0,1},{1,0},{2,3},{3,2},{4,5},{5,4},{6,7},{7,6},{8,9},{9,8},{10,11... | collective-permute-start | bytes 3145736 | tf_op jit(solution)/shard_map/ppermute | solution.py:77
  34.2 30.3 %collective-permute-start.5 = (bf16[256,2560]{1,0:T(8,128)(2,1)}, bf16[256,2560]{1,0:T(8,128)(2,1)}, u32[]{:S(2)}, u32[]{:S(2)}) collective-permute-start(bf16[256,2560]{1,0:T(8,128)(2,1)} %collective-permute-done.3), channel_id=1, source_target_pairs={{0,8},{8,16},{16,24},{24,28},{28,20},{20,12},{12,4},{4,0},{1,9},{9... | collective-permute-start | bytes 3932168 | tf_op jit(solution)/shard_map/ppermute | solution.py:46
  36.0 30.0 %collective-permute-start.6 = (bf16[256,2560]{1,0:T(8,128)(2,1)}, bf16[256,2560]{1,0:T(8,128)(2,1)S(1)}, u32[]{:S(2)}, u32[]{:S(2)}) collective-permute-start(bf16[256,2560]{1,0:T(8,128)(2,1)} %collective-permute-done.4), channel_id=1, source_target_pairs={{8,0},{16,8},{24,16},{28,24},{20,28},{12,20},{4,12},{0,4},{9,1},{1... | collective-permute-start | bytes 3932168 | tf_op jit(solution)/shard_map/ppermute | solution.py:47
  64.5 29.3 %collective-permute-start.7 = (bf16[256,2560]{1,0:T(8,128)(2,1)}, bf16[256,2560]{1,0:T(8,128)(2,1)S(1)}, u32[]{:S(2)}, u32[]{:S(2)}) collective-permute-start(bf16[256,2560]{1,0:T(8,128)(2,1)} %collective-permute-done.5), channel_id=1, source_target_pairs={{0,8},{8,16},{16,24},{24,28},{28,20},{20,12},{12,4},{4,0},{1,9},{9... | collective-permute-start | bytes 3932168 | tf_op jit(solution)/shard_map/ppermute | solution.py:46
  66.0 29.2 %collective-permute-start.8 = (bf16[256,2560]{1,0:T(8,128)(2,1)S(1)}, bf16[256,2560]{1,0:T(8,128)(2,1)S(1)}, u32[]{:S(2)}, u32[]{:S(2)}) collective-permute-start(bf16[256,2560]{1,0:T(8,128)(2,1)S(1)} %collective-permute-done.6), channel_id=1, source_target_pairs={{8,0},{16,8},{24,16},{28,24},{20,28},{12,20},{4,12},{0,4},{9,1},{1... | collective-permute-start | bytes 3932168 | tf_op jit(solution)/shard_map/ppermute | solution.py:47
  123.8 17.1 %collective-permute-start.13 = (bf16[256,1280]{1,0:T(8,128)(2,1)S(1)}, bf16[256,1280]{1,0:T(8,128)(2,1)S(1)}, u32[]{:S(2)}, u32[]{:S(2)}) collective-permute-start(bf16[256,1280]{1,0:T(8,128)(2,1)S(1)} %collective-permute-done.11), channel_id=1, source_target_pairs={{0,8},{8,16},{16,24},{24,28},{28,20},{20,12},{12,4},{4,0},{1,9},{9... | collective-permute-start | bytes 1966088 | tf_op jit(solution)/shard_map/ppermute | solution.py:46
  188.3 25.7 %collective-permute-start.25 = (bf16[256,2048]{1,0:T(8,128)(2,1)S(1)}, bf16[256,2048]{1,0:T(8,128)(2,1)}, u32[]{:S(2)}, u32[]{:S(2)}) collective-permute-start(bf16[256,2048]{1,0:T(8,128)(2,1)S(1)} %pad_maximum_fusion.1), channel_id=1, source_target_pairs={{0,8},{8,16},{16,24},{24,28},{28,20},{20,12},{12,4},{4,0},{1,9},{9... | collective-permute-start | bytes 3145736 | tf_op jit(solution)/shard_map/ppermute | solution.py:46
  190.5 25.7 %collective-permute-start.26 = (bf16[256,2048]{1,0:T(8,128)(2,1)S(1)}, bf16[256,2048]{1,0:T(8,128)(2,1)}, u32[]{:S(2)}, u32[]{:S(2)}) collective-permute-start(bf16[256,2048]{1,0:T(8,128)(2,1)S(1)} %pad_maximum_fusion.1), channel_id=1, source_target_pairs={{8,0},{16,8},{24,16},{28,24},{20,28},{12,20},{4,12},{0,4},{9,1},{1... | collective-permute-start | bytes 3145736 | tf_op jit(solution)/shard_map/ppermute | solution.py:47
  190.5 28.5 %collective-permute-start.19 = (bf16[1024,512]{1,0:T(8,128)(2,1)}, bf16[1024,512]{1,0:T(8,128)(2,1)}, u32[]{:S(2)}, u32[]{:S(2)}) collective-permute-start(bf16[1024,512]{1,0:T(8,128)(2,1)} %get-tuple-element.21), channel_id=1, source_target_pairs={{0,1},{1,0},{2,3},{3,2},{4,5},{5,4},{6,7},{7,6},{8,9},{9,8},{10,11... | collective-permute-start | bytes 3145736 | tf_op jit(solution)/shard_map/ppermute | solution.py:95
  194.1 25.5 %collective-permute-start.21 = (bf16[1024,512]{1,0:T(8,128)(2,1)}, bf16[1024,512]{1,0:T(8,128)(2,1)}, u32[]{:S(2)}, u32[]{:S(2)}) collective-permute-start(bf16[1024,512]{1,0:T(8,128)(2,1)} %add_convert_fusion.5), channel_id=1, source_target_pairs={{0,2},{1,3},{2,0},{3,1},{4,6},{5,7},{6,4},{7,5},{8,10},{9,11},{10,... | collective-permute-start | bytes 3145736 | tf_op jit(solution)/shard_map/ppermute | solution.py:100
  214.0 25.0 %collective-permute-start.27 = (bf16[256,2048]{1,0:T(8,128)(2,1)}, bf16[256,2048]{1,0:T(8,128)(2,1)}, u32[]{:S(2)}, u32[]{:S(2)}) collective-permute-start(bf16[256,2048]{1,0:T(8,128)(2,1)} %collective-permute-done.25), channel_id=1, source_target_pairs={{0,8},{8,16},{16,24},{24,28},{28,20},{20,12},{12,4},{4,0},{1,9},{9... | collective-permute-start | bytes 3145736 | tf_op jit(solution)/shard_map/ppermute | solution.py:46
  216.1 25.0 %collective-permute-start.28 = (bf16[256,2048]{1,0:T(8,128)(2,1)}, bf16[256,2048]{1,0:T(8,128)(2,1)}, u32[]{:S(2)}, u32[]{:S(2)}) collective-permute-start(bf16[256,2048]{1,0:T(8,128)(2,1)} %collective-permute-done.26), channel_id=1, source_target_pairs={{8,0},{16,8},{24,16},{28,24},{20,28},{12,20},{4,12},{0,4},{9,1},{1... | collective-permute-start | bytes 3145736 | tf_op jit(solution)/shard_map/ppermute | solution.py:47
  222.6 42.9 %collective-permute-start.23 = (bf16[1024,512]{1,0:T(8,128)(2,1)S(1)}, bf16[1024,512]{1,0:T(8,128)(2,1)S(1)}, u32[]{:S(2)}, u32[]{:S(2)}) collective-permute-start(bf16[1024,512]{1,0:T(8,128)(2,1)S(1)} %get-tuple-element.16), channel_id=1, source_target_pairs={{0,2},{1,3},{2,0},{3,1},{4,6},{5,7},{6,4},{7,5},{8,10},{9,11},{10,... | collective-permute-start | bytes 3145736 | tf_op jit(solution)/shard_map/ppermute | solution.py:72
  239.1 24.0 %collective-permute-start.29 = (bf16[256,2048]{1,0:T(8,128)(2,1)}, bf16[256,2048]{1,0:T(8,128)(2,1)S(1)}, u32[]{:S(2)}, u32[]{:S(2)}) collective-permute-start(bf16[256,2048]{1,0:T(8,128)(2,1)} %collective-permute-done.27), channel_id=1, source_target_pairs={{0,8},{8,16},{16,24},{24,28},{28,20},{20,12},{12,4},{4,0},{1,9},{9... | collective-permute-start | bytes 3145736 | tf_op jit(solution)/shard_map/ppermute | solution.py:46
  241.1 24.1 %collective-permute-start.30 = (bf16[256,2048]{1,0:T(8,128)(2,1)}, bf16[256,2048]{1,0:T(8,128)(2,1)S(1)}, u32[]{:S(2)}, u32[]{:S(2)}) collective-permute-start(bf16[256,2048]{1,0:T(8,128)(2,1)} %collective-permute-done.28), channel_id=1, source_target_pairs={{8,0},{16,8},{24,16},{28,24},{20,28},{12,20},{4,12},{0,4},{9,1},{1... | collective-permute-start | bytes 3145736 | tf_op jit(solution)/shard_map/ppermute | solution.py:47
  242.3 23.4 %collective-permute-start.22 = (bf16[1024,512]{1,0:T(8,128)(2,1)S(1)}, bf16[1024,512]{1,0:T(8,128)(2,1)S(1)}, u32[]{:S(2)}, u32[]{:S(2)}) collective-permute-start(bf16[1024,512]{1,0:T(8,128)(2,1)S(1)} %get-tuple-element.16), channel_id=1, source_target_pairs={{0,1},{1,0},{2,3},{3,2},{4,5},{5,4},{6,7},{7,6},{8,9},{9,8},{10,11... | collective-permute-start | bytes 3145736 | tf_op jit(solution)/shard_map/ppermute | solution.py:77
  314.2 31.3 %collective-permute-start.39 = (bf16[256,2560]{1,0:T(8,128)(2,1)S(1)}, bf16[256,2560]{1,0:T(8,128)(2,1)}, u32[]{:S(2)}, u32[]{:S(2)}) collective-permute-start(bf16[256,2560]{1,0:T(8,128)(2,1)S(1)} %pad_maximum_fusion), channel_id=1, source_target_pairs={{0,8},{8,16},{16,24},{24,28},{28,20},{20,12},{12,4},{4,0},{1,9},{9... | collective-permute-start | bytes 3932168 | tf_op jit(solution)/shard_map/ppermute | solution.py:46
  316.0 31.3 %collective-permute-start.40 = (bf16[256,2560]{1,0:T(8,128)(2,1)S(1)}, bf16[256,2560]{1,0:T(8,128)(2,1)}, u32[]{:S(2)}, u32[]{:S(2)}) collective-permute-start(bf16[256,2560]{1,0:T(8,128)(2,1)S(1)} %pad_maximum_fusion), channel_id=1, source_target_pairs={{8,0},{16,8},{24,16},{28,24},{20,28},{12,20},{4,12},{0,4},{9,1},{1... | collective-permute-start | bytes 3932168 | tf_op jit(solution)/shard_map/ppermute | solution.py:47
  316.4 33.4 %collective-permute-start.33 = (bf16[1024,512]{1,0:T(8,128)(2,1)S(1)}, bf16[1024,512]{1,0:T(8,128)(2,1)}, u32[]{:S(2)}, u32[]{:S(2)}) collective-permute-start(bf16[1024,512]{1,0:T(8,128)(2,1)S(1)} %get-tuple-element.19), channel_id=1, source_target_pairs={{0,1},{1,0},{2,3},{3,2},{4,5},{5,4},{6,7},{7,6},{8,9},{9,8},{10,11... | collective-permute-start | bytes 3145736 | tf_op jit(solution)/shard_map/ppermute | solution.py:95
  318.9 30.9 %collective-permute-start.35 = (bf16[1024,512]{1,0:T(8,128)(2,1)}, bf16[1024,512]{1,0:T(8,128)(2,1)}, u32[]{:S(2)}, u32[]{:S(2)}) collective-permute-start(bf16[1024,512]{1,0:T(8,128)(2,1)} %add_convert_fusion.3), channel_id=1, source_target_pairs={{0,2},{1,3},{2,0},{3,1},{4,6},{5,7},{6,4},{7,5},{8,10},{9,11},{10,... | collective-permute-start | bytes 3145736 | tf_op jit(solution)/shard_map/ppermute | solution.py:100
  345.5 30.6 %collective-permute-start.41 = (bf16[256,2560]{1,0:T(8,128)(2,1)}, bf16[256,2560]{1,0:T(8,128)(2,1)}, u32[]{:S(2)}, u32[]{:S(2)}) collective-permute-start(bf16[256,2560]{1,0:T(8,128)(2,1)} %collective-permute-done.39), channel_id=1, source_target_pairs={{0,8},{8,16},{16,24},{24,28},{28,20},{20,12},{12,4},{4,0},{1,9},{9... | collective-permute-start | bytes 3932168 | tf_op jit(solution)/shard_map/ppermute | solution.py:46
  347.2 30.6 %collective-permute-start.42 = (bf16[256,2560]{1,0:T(8,128)(2,1)}, bf16[256,2560]{1,0:T(8,128)(2,1)}, u32[]{:S(2)}, u32[]{:S(2)}) collective-permute-start(bf16[256,2560]{1,0:T(8,128)(2,1)} %collective-permute-done.40), channel_id=1, source_target_pairs={{8,0},{16,8},{24,16},{28,24},{20,28},{12,20},{4,12},{0,4},{9,1},{1... | collective-permute-start | bytes 3932168 | tf_op jit(solution)/shard_map/ppermute | solution.py:47
  352.8 29.8 %collective-permute-start.36 = (bf16[1024,512]{1,0:T(8,128)(2,1)S(1)}, bf16[1024,512]{1,0:T(8,128)(2,1)S(1)}, u32[]{:S(2)}, u32[]{:S(2)}) collective-permute-start(bf16[1024,512]{1,0:T(8,128)(2,1)S(1)} %get-tuple-element.14), channel_id=1, source_target_pairs={{0,1},{1,0},{2,3},{3,2},{4,5},{5,4},{6,7},{7,6},{8,9},{9,8},{10,11... | collective-permute-start | bytes 3145736 | tf_op jit(solution)/shard_map/ppermute | solution.py:77
  352.9 29.6 %collective-permute-start.37 = (bf16[1024,512]{1,0:T(8,128)(2,1)S(1)}, bf16[1024,512]{1,0:T(8,128)(2,1)S(1)}, u32[]{:S(2)}, u32[]{:S(2)}) collective-permute-start(bf16[1024,512]{1,0:T(8,128)(2,1)S(1)} %get-tuple-element.14), channel_id=1, source_target_pairs={{0,2},{1,3},{2,0},{3,1},{4,6},{5,7},{6,4},{7,5},{8,10},{9,11},{10,... | collective-permute-start | bytes 3145736 | tf_op jit(solution)/shard_map/ppermute | solution.py:72
  376.1 29.7 %collective-permute-start.43 = (bf16[256,2560]{1,0:T(8,128)(2,1)}, bf16[256,2560]{1,0:T(8,128)(2,1)S(1)}, u32[]{:S(2)}, u32[]{:S(2)}) collective-permute-start(bf16[256,2560]{1,0:T(8,128)(2,1)} %collective-permute-done.41), channel_id=1, source_target_pairs={{0,8},{8,16},{16,24},{24,28},{28,20},{20,12},{12,4},{4,0},{1,9},{9... | collective-permute-start | bytes 3932168 | tf_op jit(solution)/shard_map/ppermute | solution.py:46
  377.9 29.8 %collective-permute-start.44 = (bf16[256,2560]{1,0:T(8,128)(2,1)}, bf16[256,2560]{1,0:T(8,128)(2,1)S(1)}, u32[]{:S(2)}, u32[]{:S(2)}) collective-permute-start(bf16[256,2560]{1,0:T(8,128)(2,1)} %collective-permute-done.42), channel_id=1, source_target_pairs={{8,0},{16,8},{24,16},{28,24},{20,28},{12,20},{4,12},{0,4},{9,1},{1... | collective-permute-start | bytes 3932168 | tf_op jit(solution)/shard_map/ppermute | solution.py:47
  382.5 39.6 %collective-permute-start.38 = (bf16[1024,512]{1,0:T(8,128)(2,1)S(1)}, bf16[1024,512]{1,0:T(8,128)(2,1)S(1)}, u32[]{:S(2)}, u32[]{:S(2)}) collective-permute-start(bf16[1024,512]{1,0:T(8,128)(2,1)S(1)} %collective-permute-done.37), channel_id=1, source_target_pairs={{0,1},{1,0},{2,3},{3,2},{4,5},{5,4},{6,7},{7,6},{8,9},{9,8},{10,11... | collective-permute-start | bytes 3145736 | tf_op jit(solution)/shard_map/ppermute | solution.py:77
  461.4 25.3 %collective-permute-start.49 = (bf16[1024,512]{1,0:T(8,128)(2,1)S(1)}, bf16[1024,512]{1,0:T(8,128)(2,1)S(1)}, u32[]{:S(2)}, u32[]{:S(2)}) collective-permute-start(bf16[1024,512]{1,0:T(8,128)(2,1)S(1)} %add_convert_fusion.1), channel_id=1, source_target_pairs={{0,2},{1,3},{2,0},{3,1},{4,6},{5,7},{6,4},{7,5},{8,10},{9,11},{10,... | collective-permute-start | bytes 3145736 | tf_op jit(solution)/shard_map/ppermute | solution.py:100
  (47 other events, 1077.1 us)
